TPU v7x, 32 devices: a whole 2x2x4 slice. The times are simulated.
32 devices in a mesh: grp: 2 (over y), fs: 4 (over z), tp: 4 (over x, core).
Axes of the slice: x: 2, y: 2, z: 4, core: 2. Of those that a mesh axis runs over, the one named last changes fastest.
Arguments:
- tokens: bfloat16 [2048, 2048], P(('grp', 'fs'), 'tp'), parts along dimension 0, may hold values from -6 to 6
- recurrent_norm_gain: float32 [2048], replicated, may hold values from 0.1 to 1.9
- feedforward_norm_gain: float32 [2048], replicated, may hold values from 0.1 to 1.9
- gate_projection_weight: bfloat16 [2048, 2048], P('fs', 'tp'), may hold values from -0.125 to 0.125
- recurrent_projection_weight: bfloat16 [2048, 2048], P('fs', 'tp'), may hold values from -0.125 to 0.125
- convolution_kernel: bfloat16 [4, 2048], P(None, 'tp'), may hold values from -3 to 3
- decay_gate_matrix: bfloat16 [16, 128, 128], P('tp'), may hold values from -0.5 to 0.5
- input_gate_matrix: bfloat16 [16, 128, 128], P('tp'), may hold values from -0.5 to 0.5
- base_decay_logit: float32 [2048], P('tp'), may hold values from 3 to 9
- extra_log_decay: float32 [2048], P(('grp', 'fs')), parts along dimension 0, may hold values from -0.7 to 0
- output_projection_weight: bfloat16 [2048, 2048], P('tp', 'fs'), may hold values from -0.125 to 0.125
- up_projection_weight: bfloat16 [2048, 8192], P('fs', 'tp'), may hold values from -0.125 to 0.125
- down_projection_weight: bfloat16 [8192, 2048], P('tp', 'fs'), may hold values from -0.0625 to 0.0625
Outputs:
- layer_out: bfloat16 [2048, 2048], P(('grp', 'fs'), 'tp'), parts along dimension 0
There are 2 independent parts, one for each index of `grp`. A program takes and returns all parts, laid end to end along the dimension named above; an argument that names none is the same for every part. Nothing has to cross between parts.
All inputs are finite; a program needn't handle non-finite values.
Results may differ from a plain program's by a relative error of at most 0.018.
Values may be sent and summed in bfloat16 or wider, within the bound.
A program may use at most 64 MiB of HBM per device.

v0:
```python
import jax
import jax.numpy as jnp
from jax import lax
from jax.sharding import PartitionSpec as P


def rms_rows(values_in, norm_gain):
    values = values_in.astype(jnp.float32)
    inverse = lax.rsqrt(jnp.mean(values * values, axis=-1, keepdims=True) + 1e-06)
    return (values * inverse * norm_gain).astype(jnp.bfloat16)


def combine(earlier, later):
    return (earlier[0] * later[0], later[0] * earlier[1] + later[1])


def recurrent_state(
    recurrent_branch_rows,
    gate_branch_rows,
    convolution_kernel,
    decay_gate_matrix,
    input_gate_matrix,
    base_decay_logit,
    extra_log_decay,
):
    length = recurrent_branch_rows.shape[0]
    taps = convolution_kernel.shape[0]
    padded = jnp.pad(recurrent_branch_rows.astype(jnp.float32), ((taps - 1, 0), (0, 0)))
    conv_sum = jnp.zeros((length, recurrent_branch_rows.shape[1]), jnp.float32)
    for tap_index in range(taps):
        conv_sum = conv_sum + padded[tap_index : tap_index + length] * convolution_kernel[
            tap_index
        ].astype(jnp.float32)
    conv_rows = conv_sum.astype(jnp.bfloat16)
    blocks = decay_gate_matrix.shape[0]
    blocked = conv_rows.reshape(length, blocks, -1)
    recurrence_gate = jax.nn.sigmoid(
        jnp.einsum(
            "tni,nij->tnj", blocked, decay_gate_matrix, preferred_element_type=jnp.float32
        ).reshape(length, -1)
    )
    input_rate = jax.nn.sigmoid(
        jnp.einsum(
            "tni,nij->tnj", blocked, input_gate_matrix, preferred_element_type=jnp.float32
        ).reshape(length, -1)
    )
    decay_log_values = (
        -8.0 * jax.nn.softplus(-base_decay_logit) * recurrence_gate + extra_log_decay[:, None]
    )
    decay = jnp.exp(decay_log_values)
    drive = (
        jnp.sqrt(-jnp.expm1(2.0 * decay_log_values)) * input_rate * conv_rows.astype(jnp.float32)
    )
    _, hidden = lax.associative_scan(combine, (decay, drive), axis=0)
    return (hidden * gate_branch_rows.astype(jnp.float32)).astype(jnp.bfloat16)


def per_device(
    tokens,
    recurrent_norm_gain,
    feedforward_norm_gain,
    gate_projection_weight,
    recurrent_projection_weight,
    convolution_kernel,
    decay_gate_matrix,
    input_gate_matrix,
    base_decay_logit,
    extra_log_decay,
    output_projection_weight,
    up_projection_weight,
    down_projection_weight,
):
    whole_rows = lax.all_gather(tokens, "tp", axis=1, tiled=True)
    normed = rms_rows(whole_rows, recurrent_norm_gain)
    columns = normed
    gate_pre = jnp.dot(
        columns,
        lax.all_gather(gate_projection_weight, "fs", axis=0, tiled=True),
        preferred_element_type=jnp.float32,
    )
    recur_pre = jnp.dot(
        columns,
        lax.all_gather(recurrent_projection_weight, "fs", axis=0, tiled=True),
        preferred_element_type=jnp.float32,
    )
    gate_branch_rows = jax.nn.gelu(gate_pre).astype(jnp.bfloat16)
    recurrent_branch_rows = recur_pre.astype(jnp.bfloat16)
    mixed_output = recurrent_state(
        recurrent_branch_rows,
        gate_branch_rows,
        convolution_kernel,
        decay_gate_matrix,
        input_gate_matrix,
        base_decay_logit,
        extra_log_decay,
    )
    partials = jnp.dot(
        mixed_output,
        lax.all_gather(output_projection_weight, "fs", axis=1, tiled=True),
        preferred_element_type=jnp.float32,
    )
    residual = (
        tokens.astype(jnp.float32)
        + lax.psum_scatter(
            partials.astype(jnp.bfloat16), "tp", scatter_dimension=1, tiled=True
        ).astype(jnp.float32)
    ).astype(jnp.bfloat16)
    middle = lax.all_gather(residual, "tp", axis=1, tiled=True)
    channel_in = rms_rows(middle, feedforward_norm_gain)
    columns = channel_in
    upward = jnp.dot(
        columns,
        lax.all_gather(up_projection_weight, "fs", axis=0, tiled=True),
        preferred_element_type=jnp.float32,
    )
    positive = jnp.maximum(upward, 0.0)
    squared = (positive * positive).astype(jnp.bfloat16)
    down_terms = jnp.dot(
        squared,
        lax.all_gather(down_projection_weight, "fs", axis=1, tiled=True),
        preferred_element_type=jnp.float32,
    )
    summed_down = lax.psum_scatter(
        down_terms.astype(jnp.bfloat16), "tp", scatter_dimension=1, tiled=True
    ).astype(jnp.float32)
    return (residual.astype(jnp.float32) + summed_down).astype(jnp.bfloat16)


def solution(mesh):
    placed = (
        P(("grp", "fs"), "tp"),
        P(),
        P(),
        P("fs", "tp"),
        P("fs", "tp"),
        P(None, "tp"),
        P("tp", None, None),
        P("tp", None, None),
        P("tp"),
        P(("grp", "fs")),
        P("tp", "fs"),
        P("fs", "tp"),
        P("tp", "fs"),
    )
    return jax.shard_map(
        per_device, mesh=mesh, in_specs=placed, out_specs=P(("grp", "fs"), "tp"), check_vma=False
    )
```

profile of v0, /device:TPU:0, one launch (start us, length us, event | category | flops | bytes accessed | tf_op | source)
XLA Modules:
  0.0 558.3 jit_solution(17213416898491841167)
XLA Ops:
  6.5 0.7 all-gather.8.cloned.1.call-update
  7.3 0.7 all-gather.10.cloned.1.call-update
  8.1 0.7 all-gather.12.cloned.1.call-update
  8.8 0.5 all-gather.14.cloned.1.call-update
  9.4 0.8 slice_convert_fusion.3
  10.2 0.7 fusion.55
  10.9 17.4 %all-gather.8.cloned.1.call-done = bf16[256,2048]{1,0:T(8,128)(2,1)} async-done(((bf16[256,512]{1,0:T(8,128)(2,1)}), bf16[256,2048]{1,0:T(8,128)(2,1)}) %all-gather.8.cloned.1.call-update) | async-done | bytes 1048592 | tf_op jit(solution)/shard_map/all_gather | solution.py:73
  28.4 1.5 fusion.2
  29.9 45.7 %all-gather.10.cloned.1.call-done = bf16[2048,512]{1,0:T(8,128)(2,1)} async-done(((bf16[512,512]{1,0:T(8,128)(2,1)}), bf16[2048,512]{1,0:T(8,128)(2,1)}) %all-gather.10.cloned.1.call-update) | async-done | bytes 2097168 | tf_op jit(solution)/shard_map/all_gather | solution.py:83
  75.6 2.7 fusion.14
  78.3 0.2 fusion.77
  78.6 0.3 fusion.11
  78.9 0.2 copy.22
  79.1 0.1 copy-done.5
  79.2 0.3 fusion.13
  79.5 0.2 copy.23
  79.8 0.7 fusion.29
  80.4 0.3 slice.215
  80.8 0.3 slice.216
  81.1 0.3 slice.214
  81.4 0.3 slice.218
  81.7 0.1 fusion.62
  81.8 0.1 slice.221
  82.0 0.1 slice.222
  82.1 0.1 slice.220
  82.2 0.1 slice.224
  83.1 0.2 slice.219
  83.3 0.2 slice.268
  83.5 0.3 slice.270
  83.9 0.3 slice.213
  84.9 0.1 pad.69
  85.0 0.1 fusion.41
  85.1 0.1 pad.68
  85.2 36.4 %all-gather.12.cloned.1.call-done = bf16[2048,512]{1,0:T(8,128)(2,1)} async-done(((bf16[512,512]{1,0:T(8,128)(2,1)}), bf16[2048,512]{1,0:T(8,128)(2,1)}) %all-gather.12.cloned.1.call-update) | async-done | bytes 2097168 | tf_op jit(solution)/shard_map/all_gather | solution.py:78
  121.7 45.9 %all-gather.14.cloned.1.call-done = bf16[512,2048]{1,0:T(8,128)(2,1)} async-done(((bf16[512,512]{1,0:T(8,128)(2,1)}), bf16[512,2048]{1,0:T(8,128)(2,1)}) %all-gather.14.cloned.1.call-update) | async-done | bytes 2097168 | tf_op jit(solution)/shard_map/all_gather | solution.py:99
  167.6 4.8 convolution_convert_fusion
  172.4 0.0 all-gather.16.cloned.1.call-start
  172.5 23.7 %reduce-scatter.3.cloned.1.call-done = bf16[256,512]{1,0:T(8,128)(2,1)} async-done(((bf16[256,2048]{1,0:T(8,128)(2,1)}), bf16[256,512]{1,0:T(8,128)(2,1)}) %reduce-scatter.3.cloned.1.call-update) | async-done | bytes 262160 | tf_op jit(solution)/shard_map/reduce_scatter | solution.py:104
  196.1 1.7 add_convert_fusion.1
  197.9 0.7 all-gather.18.cloned.1.call-update
  198.7 0.7 all-gather.20.cloned.1.call-update
  199.4 15.3 %all-gather.16.cloned.1.call-done = bf16[256,2048]{1,0:T(8,128)(2,1)} async-done(((bf16[256,512]{1,0:T(8,128)(2,1)}), bf16[256,2048]{1,0:T(8,128)(2,1)}) %all-gather.16.cloned.1.call-update) | async-done | bytes 1048592 | tf_op jit(solution)/shard_map/all_gather | solution.py:108
  214.7 1.5 fusion.5
  216.3 149.7 %all-gather.18.cloned.1.call-done = bf16[2048,2048]{1,0:T(8,128)(2,1)} async-done(((bf16[512,2048]{1,0:T(8,128)(2,1)}), bf16[2048,2048]{1,0:T(8,128)(2,1)}) %all-gather.18.cloned.1.call-update) | async-done | bytes 8388624 | tf_op jit(solution)/shard_map/all_gather | solution.py:113
  366.0 149.4 %all-gather.20.cloned.1.call-done = bf16[2048,2048]{1,0:T(8,128)(2,1)} async-done(((bf16[2048,512]{1,0:T(8,128)(2,1)}), bf16[2048,2048]{1,0:T(8,128)(2,1)}) %all-gather.20.cloned.1.call-update) | async-done | bytes 8388624 | tf_op jit(solution)/shard_map/all_gather | solution.py:120
  515.4 11.6 %convolution_convert_fusion.1 = bf16[256,2048]{1,0:T(8,128)(2,1)} fusion(bf16[2048,2048]{1,0:T(8,128)(2,1)} %all-gather.20.cloned.1.call-done, bf16[2048,2048]{1,0:T(8,128)(2,1)} %all-gather.18.cloned.1.call-done, bf16[256,2048]{1,0:T(8,128)(2,1)} %all-gather.16.cloned.1.call-done, f32[2048]{0:T(1024)S(1)} %copy-done.7, f32[256]{0:T(256)S(1)} %add_rsqrt_fusion), kind=kOutput, calls=%fused_computation.8 | convolution fusion | flops 4299161600 | bytes 18883584 | tf_op jit(solution)/shard_map/dot_general | solution.py:118
  527.0 23.1 %reduce-scatter.5.cloned.1.call-done = bf16[256,512]{1,0:T(8,128)(2,1)} async-done(((bf16[256,2048]{1,0:T(8,128)(2,1)}), bf16[256,512]{1,0:T(8,128)(2,1)}) %reduce-scatter.5.cloned.1.call-update) | async-done | bytes 262160 | tf_op jit(solution)/shard_map/reduce_scatter | solution.py:123
  550.1 1.7 add_convert_fusion
  (101 shorter events, 1.6 us)
Async XLA Ops:
  6.5 72.0 %copy-start = (bf16[4,128,128]{2,1,0:T(8,128)(2,1)S(1)}, bf16[4,128,128]{2,1,0:T(8,128)(2,1)}, u32[]{:S(2)}) copy-start(bf16[4,128,128]{2,1,0:T(8,128)(2,1)} %param.19) | copy-start | bytes 393220
  6.5 69.1 %copy-start.6 = (f32[2048]{0:T(1024)S(1)}, f32[2048]{0:T(1024)}, u32[]{:S(2)}) copy-start(f32[2048]{0:T(1024)} %param.14) | copy-start | bytes 24580
  6.5 21.8 %all-gather.8.cloned.1.call-start = ((), (), s32[]{:S(2)}) async-start(), calls=%async_computation.2 | async-start | bytes 1310720 | tf_op jit(solution)/shard_map/all_gather | solution.py:73
  7.3 68.3 %all-gather.10.cloned.1.call-start = ((), (), s32[]{:S(2)}) async-start(), calls=%async_computation.3 | async-start | bytes 2621440 | tf_op jit(solution)/shard_map/all_gather | solution.py:83
  8.0 113.7 %all-gather.12.cloned.1.call-start = ((), (), s32[]{:S(2)}) async-start(), calls=%async_computation.4 | async-start | bytes 2621440 | tf_op jit(solution)/shard_map/all_gather | solution.py:78
  8.7 158.9 %all-gather.14.cloned.1.call-start = ((), (), s32[]{:S(2)}) async-start(), calls=%async_computation.5 | async-start | bytes 2621440 | tf_op jit(solution)/shard_map/all_gather | solution.py:99
  9.3 186.8 %reduce-scatter.3.cloned.1.call-start = ((), (), s32[]{:S(2)}) async-start(), calls=%async_computation.6 | async-start | bytes 1310720 | tf_op jit(solution)/shard_map/reduce_scatter | solution.py:104
  78.3 0.9 copy-start.5
  78.9 0.8 copy-start.4
  84.9 82.7 %copy-start.3 = (bf16[256,2048]{1,0:T(8,128)(2,1)S(1)}, bf16[256,2048]{1,0:T(8,128)(2,1)}, u32[]{:S(2)}) copy-start(bf16[256,2048]{1,0:T(8,128)(2,1)} %all-gather.8.cloned.1.call-done) | copy-start | bytes 3145732
  85.2 110.9 %copy-start.2 = (bf16[256,512]{1,0:T(8,128)(2,1)S(1)}, bf16[256,512]{1,0:T(8,128)(2,1)}, u32[]{:S(2)}) copy-start(bf16[256,512]{1,0:T(8,128)(2,1)} %param.13) | copy-start | bytes 786436
  172.4 42.3 %all-gather.16.cloned.1.call-start = ((), (), s32[]{:S(2)}) async-start(), calls=%async_computation.7 | async-start | bytes 1310720 | tf_op jit(solution)/shard_map/all_gather | solution.py:108
  197.9 168.1 %all-gather.18.cloned.1.call-start = ((), (), s32[]{:S(2)}) async-start(), calls=%async_computation.8 | async-start | bytes 10485760 | tf_op jit(solution)/shard_map/all_gather | solution.py:113
  198.6 316.7 %copy-start.7 = (f32[2048]{0:T(1024)S(1)}, f32[2048]{0:T(1024)}, u32[]{:S(2)}) copy-start(f32[2048]{0:T(1024)} %param.15) | copy-start | bytes 24580
  198.6 316.7 %all-gather.20.cloned.1.call-start = ((), (), s32[]{:S(2)}) async-start(), calls=%async_computation.9 | async-start | bytes 10485760 | tf_op jit(solution)/shard_map/all_gather | solution.py:120
  199.4 350.7 %reduce-scatter.5.cloned.1.call-start = ((), (), s32[]{:S(2)}) async-start(), calls=%async_computation.10 | async-start | bytes 1310720 | tf_op jit(solution)/shard_map/reduce_scatter | solution.py:123
  216.3 333.8 %copy-start.1 = (bf16[256,512]{1,0:T(8,128)(2,1)S(1)}, bf16[256,512]{1,0:T(8,128)(2,1)}, u32[]{:S(2)}) copy-start(bf16[256,512]{1,0:T(8,128)(2,1)} %add_convert_fusion.1) | copy-start | bytes 786436
Sparse Core Ops, SparseCore 0:
  8.9 19.4 all-gather.7
  29.9 45.6 all-gather.9
  77.2 44.4 all-gather.11
  123.1 44.4 all-gather.13
  172.5 23.5 reduce-scatter.2
  198.0 16.6 all-gather.15
  216.3 149.6 all-gather.17
  367.5 147.7 all-gather.19
  527.1 22.9 reduce-scatter.4
where the time goes:
time: 559 us; the launch traced here: 558 us
  waiting for transfers between devices  511 us (91%)
  matrix products  19.7 us (4%)
  between operations  13.8 us (2%)
  other arithmetic  9.49 us (2%)
    all_gather x1, waiting for transfers between devices, per_device(): lax.all_gather(up_projection_weight, 'fs', axis=0, tiled=True)  150 us
    all_gather x1, waiting for transfers between devices, per_device(): lax.all_gather(down_projection_weight, 'fs', axis=1, tiled=True)  149 us
    all_gather x1, waiting for transfers between devices, per_device(): lax.all_gather(output_projection_weight, 'fs', axis=1, tiled=True)  45.9 us
    all_gather x1, waiting for transfers between devices, per_device(): lax.all_gather(recurrent_projection_weight, 'fs', axis=0, tiled=True)  45.7 us
    all_gather x1, waiting for transfers between devices, per_device(): lax.all_gather(gate_projection_weight, 'fs', axis=0, tiled=True)  36.4 us
    reduce_scatter x1, waiting for transfers between devices, per_device(): lax.psum_scatter(partials.astype(jnp.bfloat16), 'tp', scatter_dimension=1...  23.7 us
    reduce_scatter x1, waiting for transfers between devices, per_device(): lax.psum_scatter(down_terms.astype(jnp.bfloat16), 'tp', scatter_dimension...  23.1 us
    all_gather x1, waiting for transfers between devices, per_device(): whole_rows = lax.all_gather(tokens, 'tp', axis=1, tiled=True)  17.4 us
  transfers between devices with their start and end apart: 9, of which 9 were waited for; matrix products, arithmetic and copies ran while one was open for 2% of the time, Pallas kernels for 0%

commit v1 on v0

--- a/solution.py
+++ b/solution.py
@@ -2,6 +2,18 @@
 import jax.numpy as jnp
 from jax import lax
 from jax.sharding import PartitionSpec as P
+
+
+def gather_by_bits(value, axis, dim):
+    ways, here, hop = (lax.axis_size(axis), lax.axis_index(axis), value.shape[dim])
+    line, have = (value, 1)
+    while have < ways:
+        line = jnp.concatenate(
+            [line, lax.ppermute(line, axis, [(d, (d - have) % ways) for d in range(ways)])],
+            axis=dim,
+        )
+        have = 2 * have
+    return jnp.roll(line, here * hop, axis=dim)
 
 
 def rms_rows(values_in, norm_gain):
@@ -74,9 +86,7 @@
     normed = rms_rows(whole_rows, recurrent_norm_gain)
     columns = normed
     gate_pre = jnp.dot(
-        columns,
-        lax.all_gather(gate_projection_weight, "fs", axis=0, tiled=True),
-        preferred_element_type=jnp.float32,
+        columns, gather_by_bits(gate_projection_weight, "fs", 0), preferred_element_type=jnp.float32
     )
     recur_pre = jnp.dot(
         columns,

time: 559 us -> 540 us (0.966)
  waiting for transfers between devices: 511 us -> 481 us
  starting transfers between devices: 0.31 us -> 6.83 us
    ppermute x0 -> x2, waiting for transfers between devices: none -> 89.6 us  [gather_by_bits(): lax.ppermute(line, axis, [(d, (d - have) % ways) for d in range(ways)])]
    all_gather x1, waiting for transfers between devices: 45.7 us -> 0.02 us  [per_device(): lax.all_gather(recurrent_projection_weight, 'fs', axis=0, tiled=True)]
    all_gather x1 -> x0, waiting for transfers between devices: 36.4 us -> none  [per_device(): lax.all_gather(gate_projection_weight, 'fs', axis=0, tiled=True)]
    all_gather x1, waiting for transfers between devices: 45.9 us -> 27.1 us  [per_device(): lax.all_gather(output_projection_weight, 'fs', axis=1, tiled=True)]
    all_gather x1, waiting for transfers between devices: 17.4 us -> 0.01 us  [per_device(): whole_rows = lax.all_gather(tokens, 'tp', axis=1, tiled=True)]
    ppermute x0 -> x2, starting transfers between devices: none -> 6.55 us  [gather_by_bits(): lax.ppermute(line, axis, [(d, (d - have) % ways) for d in range(ways)])]
  transfers between devices with their start and end apart: 9 -> 10, of which waited for: 9 -> 8; matrix products, arithmetic and copies ran while one was open for 2% -> 3% of each run, Pallas kernels for 0% -> 0%
where the time goes in v1:
time: 540 us
  waiting for transfers between devices  481 us (89%)
  matrix products  19.7 us (4%)
  between operations  14.2 us (3%)
  local copies, waits for them, and re-layouts  9.66 us (2%)
  other arithmetic  9.12 us (2%)
  starting transfers between devices  6.83 us (1%)
    all_gather x1, waiting for transfers between devices, per_device(): lax.all_gather(up_projection_weight, 'fs', axis=0, tiled=True)  150 us
    all_gather x1, waiting for transfers between devices, per_device(): lax.all_gather(down_projection_weight, 'fs', axis=1, tiled=True)  149 us
    ppermute x2, waiting for transfers between devices, gather_by_bits(): lax.ppermute(line, axis, [(d, (d - have) % ways) for d in range(ways)])  89.6 us
    all_gather x1, waiting for transfers between devices, per_device(): lax.all_gather(output_projection_weight, 'fs', axis=1, tiled=True)  27.1 us
    reduce_scatter x1, waiting for transfers between devices, per_device(): lax.psum_scatter(partials.astype(jnp.bfloat16), 'tp', scatter_dimension=1...  23.7 us
    reduce_scatter x1, waiting for transfers between devices, per_device(): lax.psum_scatter(down_terms.astype(jnp.bfloat16), 'tp', scatter_dimension...  23.1 us
    all_gather x1, waiting for transfers between devices, per_device(): middle = lax.all_gather(residual, 'tp', axis=1, tiled=True)  15.5 us
    dot_general x1, matrix products, per_device(): jnp.dot(squared, lax.all_gather(down_projection_weight, 'fs', axis=1, til...  11.6 us
  transfers between devices with their start and end apart: 10, of which 8 were waited for; matrix products, arithmetic and copies ran while one was open for 3% of the time, Pallas kernels for 0%

profile of v1, /device:TPU:0, one launch (start us, length us, event | category | flops | bytes accessed | tf_op | source)
XLA Modules:
  0.0 540.1 jit_solution(17931695784055560704)
XLA Ops:
  6.5 0.7 all-gather.7.cloned.1.call-update
  7.3 0.7 all-gather.9.cloned.1.call-update
  8.1 5.1 collective-permute-start
  13.2 11.5 %collective-permute-done = bf16[512,512]{1,0:T(8,128)(2,1)S(1)} collective-permute-done((bf16[512,512]{1,0:T(8,128)(2,1)}, bf16[512,512]{1,0:T(8,128)(2,1)S(1)}, u32[]{:S(2)}, u32[]{:S(2)}) %collective-permute-start) | collective-permute-done | bytes 524320 | tf_op jit(solution)/shard_map/ppermute | solution.py:12
  24.7 1.1 pad_maximum_fusion
  25.8 1.4 collective-permute-start.1
  27.3 0.8 constant_dynamic-update-slice_fusion.5
  28.2 0.8 constant_dynamic-update-slice_fusion.4
  29.1 78.1 %collective-permute-done.1 = bf16[1024,512]{1,0:T(8,128)(2,1)S(1)} collective-permute-done((bf16[1024,512]{1,0:T(8,128)(2,1)S(1)}, bf16[1024,512]{1,0:T(8,128)(2,1)S(1)}, u32[]{:S(2)}, u32[]{:S(2)}) %collective-permute-start.1) | collective-permute-done | bytes 1048608 | tf_op jit(solution)/shard_map/ppermute | solution.py:12
  107.2 1.0 constant_dynamic-update-slice_fusion.3
  108.2 0.8 constant_dynamic-update-slice_fusion.2
  109.1 0.8 constant_dynamic-update-slice_fusion.1
  109.9 1.0 constant_dynamic-update-slice_fusion
  110.9 1.5 fusion.2
  112.5 2.7 fusion.16
  115.2 0.2 fusion.90
  115.5 0.3 fusion.13
  115.8 0.2 copy.22
  116.1 0.3 fusion.15
  116.5 0.2 copy.23
  116.7 0.7 fusion.47
  117.3 0.3 slice.215
  117.7 0.3 slice.216
  118.0 0.3 slice.214
  118.3 0.3 slice.218
  118.7 0.1 fusion.76
  118.8 0.1 slice.221
  118.9 0.1 slice.222
  119.0 0.1 slice.220
  119.1 0.1 slice.224
  120.0 0.2 slice.219
  120.2 0.2 slice.268
  120.4 0.3 slice.270
  120.8 0.3 slice.213
  121.9 0.1 fusion.53
  122.1 27.1 %all-gather.11.cloned.1.call-done = bf16[512,2048]{1,0:T(8,128)(2,1)} async-done(((bf16[512,512]{1,0:T(8,128)(2,1)}), bf16[512,2048]{1,0:T(8,128)(2,1)}) %all-gather.11.cloned.1.call-update) | async-done | bytes 2097168 | tf_op jit(solution)/shard_map/all_gather | solution.py:109
  149.3 4.7 convolution_convert_fusion
  154.1 23.7 %reduce-scatter.3.cloned.1.call-done = bf16[256,512]{1,0:T(8,128)(2,1)} async-done(((bf16[256,2048]{1,0:T(8,128)(2,1)}), bf16[256,512]{1,0:T(8,128)(2,1)}) %reduce-scatter.3.cloned.1.call-update) | async-done | bytes 262160 | tf_op jit(solution)/shard_map/reduce_scatter | solution.py:114
  177.7 1.7 add_convert_fusion.1
  179.5 0.5 all-gather.15.cloned.1.call-update
  180.1 0.7 all-gather.17.cloned.1.call-update
  180.9 15.5 %all-gather.13.cloned.1.call-done = bf16[256,2048]{1,0:T(8,128)(2,1)} async-done(((bf16[256,512]{1,0:T(8,128)(2,1)}), bf16[256,2048]{1,0:T(8,128)(2,1)}) %all-gather.13.cloned.1.call-update) | async-done | bytes 1048592 | tf_op jit(solution)/shard_map/all_gather | solution.py:118
  196.4 1.5 fusion.5
  197.9 149.5 %all-gather.15.cloned.1.call-done = bf16[2048,2048]{1,0:T(8,128)(2,1)} async-done(((bf16[512,2048]{1,0:T(8,128)(2,1)}), bf16[2048,2048]{1,0:T(8,128)(2,1)}) %all-gather.15.cloned.1.call-update) | async-done | bytes 8388624 | tf_op jit(solution)/shard_map/all_gather | solution.py:123
  347.4 149.4 %all-gather.17.cloned.1.call-done = bf16[2048,2048]{1,0:T(8,128)(2,1)} async-done(((bf16[2048,512]{1,0:T(8,128)(2,1)}), bf16[2048,2048]{1,0:T(8,128)(2,1)}) %all-gather.17.cloned.1.call-update) | async-done | bytes 8388624 | tf_op jit(solution)/shard_map/all_gather | solution.py:130
  496.8 11.6 %convolution_convert_fusion.1 = bf16[256,2048]{1,0:T(8,128)(2,1)} fusion(bf16[2048,2048]{1,0:T(8,128)(2,1)} %all-gather.17.cloned.1.call-done, bf16[2048,2048]{1,0:T(8,128)(2,1)} %all-gather.15.cloned.1.call-done, bf16[256,2048]{1,0:T(8,128)(2,1)} %all-gather.13.cloned.1.call-done, f32[2048]{0:T(1024)S(1)} %copy-done.10, f32[256]{0:T(256)S(1)} %add_rsqrt_fusion), kind=kOutput, calls=%fused_computation.8 | convolution fusion | flops 4299161600 | bytes 18883584 | tf_op jit(solution)/shard_map/dot_general | solution.py:128
  508.4 23.1 %reduce-scatter.5.cloned.1.call-done = bf16[256,512]{1,0:T(8,128)(2,1)} async-done(((bf16[256,2048]{1,0:T(8,128)(2,1)}), bf16[256,512]{1,0:T(8,128)(2,1)}) %reduce-scatter.5.cloned.1.call-update) | async-done | bytes 262160 | tf_op jit(solution)/shard_map/reduce_scatter | solution.py:133
  531.5 1.7 add_convert_fusion
  (115 shorter events, 1.9 us)
Async XLA Ops:
  6.5 108.9 %copy-start = (bf16[4,128,128]{2,1,0:T(8,128)(2,1)S(1)}, bf16[4,128,128]{2,1,0:T(8,128)(2,1)}, u32[]{:S(2)}) copy-start(bf16[4,128,128]{2,1,0:T(8,128)(2,1)} %param.19) | copy-start | bytes 393220
  6.5 20.8 %copy-start.1 = (bf16[512,512]{1,0:T(8,128)(2,1)S(1)}, bf16[512,512]{1,0:T(8,128)(2,1)}, u32[]{:S(2)}) copy-start(bf16[512,512]{1,0:T(8,128)(2,1)} %param.16) | copy-start | bytes 1572868
  6.5 104.4 %all-gather.7.cloned.1.call-start = ((), (), s32[]{:S(2)}) async-start(), calls=%async_computation.2 | async-start | bytes 1310720 | tf_op jit(solution)/shard_map/all_gather | solution.py:85
  7.3 20.9 %copy-start.6 = (f32[512]{0:T(512)S(1)}, f32[512]{0:T(512)}, u32[]{:S(2)}) copy-start(f32[512]{0:T(512)} %param.21) | copy-start | bytes 6148
  7.3 20.9 %copy-start.5 = (bf16[4,512]{1,0:T(4,128)(2,1)S(1)}, bf16[4,512]{1,0:T(4,128)(2,1)}, u32[]{:S(2)}) copy-start(bf16[4,512]{1,0:T(4,128)(2,1)} %param.18) | copy-start | bytes 12292
  7.3 105.2 %all-gather.9.cloned.1.call-start = ((), (), s32[]{:S(2)}) async-start(), calls=%async_computation.3 | async-start | bytes 2621440 | tf_op jit(solution)/shard_map/all_gather | solution.py:93
  8.0 141.2 %all-gather.11.cloned.1.call-start = ((), (), s32[]{:S(2)}) async-start(), calls=%async_computation.4 | async-start | bytes 2621440 | tf_op jit(solution)/shard_map/all_gather | solution.py:109
  8.1 16.6 %collective-permute-start = (bf16[512,512]{1,0:T(8,128)(2,1)}, bf16[512,512]{1,0:T(8,128)(2,1)S(1)}, u32[]{:S(2)}, u32[]{:S(2)}) collective-permute-start(bf16[512,512]{1,0:T(8,128)(2,1)} %param.16), channel_id=1, source_target_pairs={{0,12},{4,0},{8,4},{12,8},{1,13},{5,1},{9,5},{13,9},{2,14},{6,2},{... | collective-permute-start | bytes 1572872 | tf_op jit(solution)/shard_map/ppermute | solution.py:12
  25.8 81.4 %collective-permute-start.1 = (bf16[1024,512]{1,0:T(8,128)(2,1)S(1)}, bf16[1024,512]{1,0:T(8,128)(2,1)S(1)}, u32[]{:S(2)}, u32[]{:S(2)}) collective-permute-start(bf16[1024,512]{1,0:T(8,128)(2,1)S(1)} %pad_maximum_fusion), channel_id=1, source_target_pairs={{0,8},{4,12},{8,0},{12,4},{1,9},{5,13},{9,1},{13,5},{2,10},{6,14},... | collective-permute-start | bytes 3145736 | tf_op jit(solution)/shard_map/ppermute | solution.py:12
  27.3 150.5 %reduce-scatter.3.cloned.1.call-start = ((), (), s32[]{:S(2)}) async-start(), calls=%async_computation.5 | async-start | bytes 1310720 | tf_op jit(solution)/shard_map/reduce_scatter | solution.py:114
  109.1 3.5 copy-start.9
  115.2 0.9 copy-start.8
  115.8 0.8 copy-start.7
  121.8 27.5 %copy-start.4 = (bf16[256,2048]{1,0:T(8,128)(2,1)S(1)}, bf16[256,2048]{1,0:T(8,128)(2,1)}, u32[]{:S(2)}) copy-start(bf16[256,2048]{1,0:T(8,128)(2,1)} %all-gather.7.cloned.1.call-done) | copy-start | bytes 3145732
  122.1 55.6 %copy-start.3 = (bf16[256,512]{1,0:T(8,128)(2,1)S(1)}, bf16[256,512]{1,0:T(8,128)(2,1)}, u32[]{:S(2)}) copy-start(bf16[256,512]{1,0:T(8,128)(2,1)} %param.13) | copy-start | bytes 786436
  154.0 42.4 %all-gather.13.cloned.1.call-start = ((), (), s32[]{:S(2)}) async-start(), calls=%async_computation.6 | async-start | bytes 1310720 | tf_op jit(solution)/shard_map/all_gather | solution.py:118
  179.5 167.9 %all-gather.15.cloned.1.call-start = ((), (), s32[]{:S(2)}) async-start(), calls=%async_computation.7 | async-start | bytes 10485760 | tf_op jit(solution)/shard_map/all_gather | solution.py:123
  180.1 316.8 %copy-start.10 = (f32[2048]{0:T(1024)S(1)}, f32[2048]{0:T(1024)}, u32[]{:S(2)}) copy-start(f32[2048]{0:T(1024)} %param.15) | copy-start | bytes 24580
  180.1 316.7 %all-gather.17.cloned.1.call-start = ((), (), s32[]{:S(2)}) async-start(), calls=%async_computation.8 | async-start | bytes 10485760 | tf_op jit(solution)/shard_map/all_gather | solution.py:130
  180.8 350.7 %reduce-scatter.5.cloned.1.call-start = ((), (), s32[]{:S(2)}) async-start(), calls=%async_computation.9 | async-start | bytes 1310720 | tf_op jit(solution)/shard_map/reduce_scatter | solution.py:133
  197.9 333.7 %copy-start.2 = (bf16[256,512]{1,0:T(8,128)(2,1)S(1)}, bf16[256,512]{1,0:T(8,128)(2,1)}, u32[]{:S(2)}) copy-start(bf16[256,512]{1,0:T(8,128)(2,1)} %add_convert_fusion.1) | copy-start | bytes 786436
Sparse Core Ops, SparseCore 0:
  8.9 19.4 all-gather.6
  29.9 73.5 all-gather.8
  105.1 44.1 all-gather.10
  154.1 23.5 reduce-scatter.2
  179.6 16.6 all-gather.12
  197.8 149.6 all-gather.14
  349.0 147.7 all-gather.16
  508.6 22.9 reduce-scatter.4
